TPU v7x, 32 devices: a whole 2x2x4 slice. The times are simulated.
32 devices in a mesh: ep: 8 (over z, y), tp: 4 (over x, core).
Axes of the slice: x: 2, y: 2, z: 4, core: 2. Of those that a mesh axis runs over, the one named last changes fastest.
Arguments:
- hidden: bfloat16 [256, 2048], P('ep')
- norm_gains: float32 [4, 2048], replicated, may hold values from 0.1 to 1.9
- w_query: bfloat16 [2048, 1024], P(None, 'tp'), may hold values from -0.125 to 0.125
- w_key: bfloat16 [2048, 1024], P(None, 'tp'), may hold values from -0.125 to 0.125
- w_value: bfloat16 [2048, 1024], P(None, 'tp'), may hold values from -0.125 to 0.125
- w_outgate: bfloat16 [2048, 1024], P(None, 'tp'), may hold values from -0.125 to 0.125
- w_input_gate: bfloat16 [2048, 8], replicated, may hold values from -0.125 to 0.125
- w_forget_gate: bfloat16 [2048, 8], replicated, may hold values from -0.125 to 0.125
- forget_bias: float32 [8], replicated, may hold values from -1 to 4
- w_mix_out: bfloat16 [1024, 2048], P('tp')
- state_matrix: float32 [256, 8, 128, 128], P('ep', 'tp'), may hold values from -0.6 to 0.6
- state_norm: float32 [256, 8, 128], P('ep', 'tp'), may hold values from -0.6 to 0.6
- state_max: float32 [256, 8], P('ep', 'tp'), may hold values from -4 to 4
- routes: int32 [256, 2], P('ep'), may hold values from 0 to 7, all different within a row; in each aligned block of 32 rows (0 to 31, 32 to 63, ...) at most 16 rows name the same one
- route_scores: float32 [256, 2], P('ep'), may hold values from 0.1 to 1
- expert_gate: bfloat16 [8, 2048, 3584], P('ep', None, 'tp'), may hold values from -0.125 to 0.125
- expert_up: bfloat16 [8, 2048, 3584], P('ep', None, 'tp'), may hold values from -0.125 to 0.125
- expert_down: bfloat16 [8, 3584, 2048], P('ep', 'tp')
- dense_gate: bfloat16 [2048, 5632], P('tp', 'ep'), may hold values from -0.125 to 0.125
- dense_up: bfloat16 [2048, 5632], P('tp', 'ep'), may hold values from -0.125 to 0.125
- dense_down: bfloat16 [5632, 2048], P('ep', 'tp')
- dense_mix: float32 [2048], replicated, may hold values from -0.25 to 0.25
Outputs:
- new_hidden: bfloat16 [256, 2048], P('ep', 'tp')
- new_matrix: float32 [256, 8, 128, 128], P('ep', 'tp')
- new_norm: float32 [256, 8, 128], P('ep', 'tp')
- new_max: float32 [256, 8], P('ep', 'tp')
Inputs may be any that keep to these rules, and one draw needn't show every extreme that they name: `routes`: each row names 2 different experts. Among the rows of one index of ep (an aligned block of 32 rows) no expert is named by more than 16 rows, and in every draw some expert is named by exactly 16 rows of some block.
All inputs are finite; a program needn't handle non-finite values.
Results may differ from a plain program's by a relative error of at most 0.02.
Values may be sent and summed in bfloat16 or wider, within the bound.
No kernel may reach another device: no remote copies, remote signals or barrier semaphores. Data moves between devices by JAX's collectives and lax.ppermute only.
A program may use at most 128 MiB of HBM per device.

v0:
```python
import jax
import jax.numpy as jnp
from jax import lax
from jax.sharding import PartitionSpec as P

EPS = 1e-06


def settle(values):
    return lax.optimization_barrier(values.astype(jnp.bfloat16)).astype(jnp.float32)


def local(
    hidden,
    norm_gains,
    w_query,
    w_key,
    w_value,
    w_outgate,
    w_input_gate,
    w_forget_gate,
    forget_bias,
    w_mix_out,
    state_matrix,
    state_norm,
    state_max,
    routes,
    route_scores,
    expert_gate,
    expert_up,
    expert_down,
    dense_gate,
    dense_up,
    dense_down,
    dense_mix,
):
    tp_count = lax.axis_size("tp")
    ep_count = lax.axis_size("ep")
    tp_place = lax.axis_index("tp")
    seq_local, width = hidden.shape
    heads_local = state_matrix.shape[1]
    head_width = state_matrix.shape[2]
    part_width = width // tp_count
    feature_first = tp_place * part_width
    start_f = hidden.astype(jnp.float32)
    normed_in = (
        start_f
        * lax.rsqrt(jnp.mean(start_f * start_f, axis=-1, keepdims=True) + EPS)
        * norm_gains[0]
    ).astype(jnp.bfloat16)
    query_f = jnp.dot(normed_in, w_query, preferred_element_type=jnp.float32)
    key_f = jnp.dot(normed_in, w_key, preferred_element_type=jnp.float32)
    value_f = jnp.dot(normed_in, w_value, preferred_element_type=jnp.float32)
    gate_f = jnp.dot(normed_in, w_outgate, preferred_element_type=jnp.float32)
    head_first = tp_place * heads_local
    input_weight = lax.dynamic_slice_in_dim(w_input_gate, head_first, heads_local, 1)
    forget_weight = lax.dynamic_slice_in_dim(w_forget_gate, head_first, heads_local, 1)
    forget_local = lax.dynamic_slice_in_dim(forget_bias, head_first, heads_local, 0)
    in_gate = jnp.dot(normed_in, input_weight, preferred_element_type=jnp.float32)
    log_forget = jax.nn.log_sigmoid(
        jnp.dot(normed_in, forget_weight, preferred_element_type=jnp.float32) + forget_local
    )
    query = settle(query_f).reshape(seq_local, heads_local, head_width)
    keys = settle(key_f).reshape(seq_local, heads_local, head_width) * head_width ** (-0.5)
    values = settle(value_f).reshape(seq_local, heads_local, head_width)
    carried = log_forget + state_max
    new_max = jnp.maximum(carried, in_gate)
    keep = jnp.exp(carried - new_max)
    write = jnp.exp(in_gate - new_max)
    written = write[:, :, None] * keys
    new_matrix = (
        keep[:, :, None, None] * state_matrix + written[:, :, :, None] * values[:, :, None, :]
    )
    new_norm = keep[:, :, None] * state_norm + written
    numer = jnp.einsum("shd,shdv->shv", query, new_matrix)
    denom = jnp.einsum("shd,shd->sh", query, new_norm)
    read = numer / jnp.maximum(jnp.abs(denom), jnp.exp(-new_max))[:, :, None]
    mixed = (
        jax.nn.sigmoid(settle(gate_f)) * read.reshape(seq_local, heads_local * head_width)
    ).astype(jnp.bfloat16)
    branch_terms = settle(jnp.dot(mixed, w_mix_out, preferred_element_type=jnp.float32))
    branch = settle(
        lax.psum_scatter(
            branch_terms.astype(jnp.bfloat16), "tp", scatter_dimension=1, tiled=True
        ).astype(jnp.float32)
    )
    start_part = lax.dynamic_slice_in_dim(start_f, feature_first, part_width, 1)
    gain_rows = lax.dynamic_slice_in_dim(norm_gains, feature_first, part_width, 1)
    lifted = gain_rows[1] * branch
    mix_weight = gain_rows[2] * lax.dynamic_slice_in_dim(dense_mix, feature_first, part_width, 0)
    branch_sq, start_sq, cross_sum, lifted_sq, start_dot, lifted_dot = lax.psum(
        (
            jnp.sum(branch * branch, axis=-1),
            jnp.sum(start_part * start_part, axis=-1),
            jnp.sum(start_part * lifted, axis=-1),
            jnp.sum(lifted * lifted, axis=-1),
            jnp.sum(start_part * mix_weight, axis=-1),
            jnp.sum(lifted * mix_weight, axis=-1),
        ),
        "tp",
    )
    branch_scale = lax.rsqrt(branch_sq / width + EPS)
    residual_f = start_part + lifted * branch_scale[:, None]
    resid_sq = start_sq + 2.0 * branch_scale * cross_sum + branch_scale * branch_scale * lifted_sq
    gate_dot = start_dot + branch_scale * lifted_dot
    scale_two = lax.rsqrt(resid_sq / width + EPS)
    mix_gate = jax.nn.sigmoid(scale_two * gate_dot)
    residual = settle(residual_f)
    normed = (residual_f * scale_two[:, None] * gain_rows[2]).astype(jnp.bfloat16)
    rows_in = lax.all_gather(normed, "ep", axis=0, tiled=True)
    dense_pre = jnp.concatenate(
        [
            jnp.dot(rows_in, dense_gate, preferred_element_type=jnp.float32),
            jnp.dot(rows_in, dense_up, preferred_element_type=jnp.float32),
        ],
        axis=1,
    )
    dense_pre = lax.psum(dense_pre.astype(jnp.bfloat16), "tp").astype(jnp.float32)
    dense_pre_gate, dense_pre_up = jnp.split(dense_pre, 2, axis=1)
    dense_hidden = (jax.nn.silu(dense_pre_gate) * dense_pre_up).astype(jnp.bfloat16)
    dense_out = lax.psum_scatter(
        jnp.dot(dense_hidden, dense_down, preferred_element_type=jnp.float32).astype(jnp.bfloat16),
        "ep",
        scatter_dimension=0,
        tiled=True,
    ).astype(jnp.float32)
    route_width = routes.shape[1]
    expert_count = ep_count * expert_gate.shape[0]
    capacity = 2 * seq_local * route_width // ep_count
    flat_expert = routes.reshape(-1)
    picks = (flat_expert[:, None] == jnp.arange(expert_count, dtype=jnp.int32)[None, :]).astype(
        jnp.int32
    )
    ranks = jnp.sum(jnp.cumsum(picks, axis=0) * picks, axis=1) - 1
    slot_index = flat_expert * capacity + ranks
    placing = (
        jnp.arange(expert_count * capacity, dtype=jnp.int32)[:, None] == slot_index[None, :]
    ).astype(jnp.bfloat16)
    repeated = jnp.repeat(normed, route_width, axis=0)
    outgoing = (
        jnp.dot(placing, repeated, preferred_element_type=jnp.float32)
        .astype(jnp.bfloat16)
        .reshape(expert_count, capacity, part_width)
    )
    arrived = lax.all_to_all(outgoing, "ep", split_axis=0, concat_axis=0, tiled=True)
    full_rows = lax.all_gather(arrived, "tp", axis=2, tiled=True)
    flat_rows = full_rows.reshape(-1, width)
    gate_pre = jnp.dot(flat_rows, expert_gate[0], preferred_element_type=jnp.float32)
    up_pre = jnp.dot(flat_rows, expert_up[0], preferred_element_type=jnp.float32)
    hidden_units = (jax.nn.silu(gate_pre) * up_pre).astype(jnp.bfloat16)
    partial_out = settle(jnp.dot(hidden_units, expert_down[0], preferred_element_type=jnp.float32))
    summed_out = lax.psum_scatter(
        partial_out.astype(jnp.bfloat16), "tp", scatter_dimension=1, tiled=True
    )
    returned = lax.all_to_all(
        summed_out.reshape(arrived.shape), "ep", split_axis=0, concat_axis=0, tiled=True
    )
    picked = lax.dot_general(
        placing,
        returned.reshape(expert_count * capacity, part_width),
        (((0,), (0,)), ((), ())),
        preferred_element_type=jnp.float32,
    )
    share = route_scores / jnp.sum(route_scores, axis=-1, keepdims=True)
    moe_out = jnp.sum(
        picked.reshape(seq_local, route_width, part_width) * share[:, :, None], axis=1
    )
    ffn = moe_out + mix_gate[:, None] * dense_out
    ffn_sq = lax.psum(jnp.sum(ffn * ffn, axis=-1), "tp")
    new_hidden = (residual + gain_rows[3] * ffn * lax.rsqrt(ffn_sq / width + EPS)[:, None]).astype(
        jnp.bfloat16
    )
    return (new_hidden, new_matrix, new_norm, new_max)


def solution(mesh):
    placed = (
        P("ep", None),
        P(),
        P(None, "tp"),
        P(None, "tp"),
        P(None, "tp"),
        P(None, "tp"),
        P(),
        P(),
        P(),
        P("tp", None),
        P("ep", "tp", None, None),
        P("ep", "tp", None),
        P("ep", "tp"),
        P("ep", None),
        P("ep", None),
        P("ep", None, "tp"),
        P("ep", None, "tp"),
        P("ep", "tp", None),
        P("tp", "ep"),
        P("tp", "ep"),
        P("ep", "tp"),
        P(),
    )
    return jax.shard_map(
        local,
        mesh=mesh,
        in_specs=placed,
        out_specs=(P("ep", "tp"), P("ep", "tp", None, None), P("ep", "tp", None), P("ep", "tp")),
        check_vma=False,
    )
```

profile of v0, /device:TPU:0, one launch (start us, length us, event | category | flops | bytes accessed | tf_op | source)
XLA Modules:
  0.0 237.0 jit_solution(14512095781934341025)
XLA Ops:
  7.2 0.0 copy-start
  7.2 0.0 copy-start.2
  7.2 0.0 reduce-scatter.4.cloned.1.call-start
  7.3 0.9 slice.14
  8.2 1.0 multiply_reduce_fusion
  9.2 1.6 convolution_convert_fusion.7
  10.9 1.1 fusion.44
  12.0 0.7 dynamic_slice.21
  12.8 1.2 subtract_exponential_fusion
  13.9 0.0 copy-start.7
  14.0 0.1 copy.32
  14.0 0.1 copy.31
  14.1 1.6 convolution_convert_fusion.6
  15.8 1.6 convolution_convert_fusion.5
  17.5 0.8 fusion.38
  18.2 0.1 copy.42
  18.3 0.1 copy.34
  18.4 0.3 convolution_convert_fusion.8
  18.7 3.7 %multiply_add_fusion = f32[32,2,128,128]{3,2,1,0:T(8,128)S(1)} fusion(f32[32,2,128,128]{3,2,1,0:T(8,128)} %param.32, f32[32,2,128]{2,1,0:T(2,128)S(1)} %reshape.112, f32[32,2,128]{2,1,0:T(2,128)S(1)} %get-tuple-element.20, f32[32,2]{1,0:T(8,128)S(1)} %copy.31), kind=kLoop, calls=%fused_computation | loop fusion | flops 3145728 | bytes 8454400 | tf_op jit(solution)/shard_map/add | solution.py:72
  22.4 0.0 copy-start.1
  22.5 2.0 copy-done.1
  24.5 0.6 fusion.57
  25.1 0.1 broadcast_divide_fusion
  25.3 0.9 convolution_convert_fusion
  26.2 0.0 reduce-scatter.4.cloned.1.call-update
  26.2 0.1 copy.35
  26.3 0.1 reshape.104
  26.4 0.1 fusion.40
  26.5 0.1 reduce_window_sum.11
  26.6 0.2 select_reduce_fusion
  26.8 0.9 fusion.56
  27.7 0.8 dynamic-slice_multiply_fusion
  28.5 20.2 %reduce-scatter.4.cloned.1.call-done = bf16[32,512]{1,0:T(8,128)(2,1)} async-done(((bf16[32,2048]{1,0:T(8,128)(2,1)}), bf16[32,512]{1,0:T(8,128)(2,1)}) %reduce-scatter.4.cloned.1.call-update) | async-done | bytes 32784 | tf_op jit(solution)/shard_map/reduce_scatter | solution.py:83
  48.7 1.0 multiply_reduce_fusion.2
  49.7 5.8 %all-reduce = (f32[32]{0:T(128)S(1)}, f32[32]{0:T(128)S(1)}, f32[32]{0:T(128)S(1)}, f32[32]{0:T(128)S(1)}, f32[32]{0:T(128)S(1)}, /*index=5*/f32[32]{0:T(128)S(1)}) all-reduce(f32[32]{0:T(128)S(1)} %get-tuple-element.9, f32[32]{0:T(128)S(1)} %get-tuple-element.8, f32[32]{0:T(128)S(1)} %get-tuple-element.5, ...), channel_id=1, replica_groups=mesh['ep'=8,'tp'=4] {'tp'}, use_global_device_ids=true, to_apply=%region_3.4 | all-reduce | flops 192 | bytes 1536 | tf_op jit(solution)/shard_map/psum | solution.py:91
  55.5 0.9 multiply_convert_fusion.1
  56.3 31.2 %all_gather.7 = bf16[256,512]{1,0:T(8,128)(2,1)S(1)} all-gather(bf16[32,512]{1,0:T(8,128)(2,1)S(1)} %get-tuple-element.23), channel_id=1, replica_groups=mesh['ep'=8,'tp'=4] {'ep'}, dimensions={0}, use_global_device_ids=true | all-gather | bytes 294912 | tf_op jit(solution)/shard_map/all_gather | solution.py:110
  87.5 0.4 convolution_convert_fusion.1
  87.9 0.4 convolution_convert_fusion.2
  88.4 0.8 convolution_convert_fusion.4
  89.2 5.3 %all-to-all-start = ((bf16[8,16,512]{2,1,0:T(8,128)(2,1)}), bf16[8,16,512]{2,1,0:T(8,128)(2,1)S(1)}, u32[]{:S(2)}, u32[]{:S(2)}) async-start(bf16[8,16,512]{2,1,0:T(8,128)(2,1)} %bitcast.6), calls=%async_computation.1 | async-start | bytes 262144 | tf_op jit(solution)/shard_map/all_to_all | solution.py:145
  94.5 0.0 all-reduce.3.cloned.1.call-start
  94.5 0.9 pad_maximum_fusion
  95.4 0.0 all-reduce.3.cloned.1.call-update
  95.5 0.0 reduce-scatter.6.cloned.1.call-start
  95.5 6.3 %all-to-all-done = bf16[8,16,512]{2,1,0:T(8,128)(2,1)S(1)} async-done(((bf16[8,16,512]{2,1,0:T(8,128)(2,1)}), bf16[8,16,512]{2,1,0:T(8,128)(2,1)S(1)}, u32[]{:S(2)}, u32[]{:S(2)}) %all-to-all-start) | async-done | bytes 131104 | tf_op jit(solution)/shard_map/all_to_all | solution.py:145
  101.8 9.2 %all_gather.6 = bf16[8,16,2048]{2,1,0:T(8,128)(2,1)S(1)} all-gather(bf16[8,16,512]{2,1,0:T(8,128)(2,1)S(1)} %all-to-all-done), channel_id=1, replica_groups=mesh['ep'=8,'tp'=4] {'tp'}, dimensions={2}, use_global_device_ids=true | all-gather | bytes 655360 | tf_op jit(solution)/shard_map/all_gather | solution.py:146
  111.0 2.8 %fusion.4 = f32[128,896]{1,0:T(8,128)S(1)} fusion(bf16[128,2048]{1,0:T(8,128)(2,1)S(1)} %bitcast.51, bf16[1,2048,896]{2,1,0:T(8,128)(2,1)} %param.37), kind=kOutput, calls=%fused_computation.5 | convolution fusion | flops 469762048 | bytes 4653056 | tf_op jit(solution)/shard_map/dot_general | solution.py:148
  113.9 5.5 %fusion.6 = bf16[128,2048]{1,0:T(8,128)(2,1)} fusion(bf16[1,896,2048]{2,1,0:T(8,128)(2,1)} %param.39, bf16[128,2048]{1,0:T(8,128)(2,1)S(1)} %bitcast.52, bf16[1,2048,896]{2,1,0:T(8,128)(2,1)} %param.38, f32[128,896]{1,0:T(8,128)S(1)} %fusion.4), kind=kOutput, calls=%fused_computation.7 | convolution fusion | flops 940474368 | bytes 8847360 | tf_op jit(solution)/shard_map/dot_general | solution.py:151
  119.3 0.0 reduce-scatter.6.cloned.1.call-update
  119.3 0.0 reduce-scatter.8.cloned.1.call-start
  119.4 13.2 %all-reduce.3.cloned.1.call-done = bf16[256,1408]{0,1:T(8,128)(2,1)} async-done(((bf16[256,1408]{0,1:T(8,128)(2,1)}), bf16[256,1408]{0,1:T(8,128)(2,1)}) %all-reduce.3.cloned.1.call-update) | async-done | bytes 720912 | tf_op jit(solution)/shard_map/psum | solution.py:118
  132.6 1.2 convert_element_type.94
  133.8 1.1 convolution_convert_fusion.3
  134.9 0.0 reduce-scatter.8.cloned.1.call-update
  134.9 21.8 %reduce-scatter.6.cloned.1.call-done = bf16[128,512]{1,0:T(8,128)(2,1)} async-done(((bf16[128,2048]{1,0:T(8,128)(2,1)}), bf16[128,512]{1,0:T(8,128)(2,1)}) %reduce-scatter.6.cloned.1.call-update) | async-done | bytes 131088 | tf_op jit(solution)/shard_map/reduce_scatter | solution.py:152
  156.7 5.5 %all-to-all-start.1 = ((bf16[8,16,512]{2,1,0:T(8,128)(2,1)}), bf16[8,16,512]{2,1,0:T(8,128)(2,1)S(1)}, u32[]{:S(2)}, u32[]{:S(2)}) async-start(bf16[8,16,512]{2,1,0:T(8,128)(2,1)} %bitcast.62), calls=%async_computation.3 | async-start | bytes 262144 | tf_op jit(solution)/shard_map/all_to_all | solution.py:155
  162.3 0.1 iota_compare_fusion.3
  162.4 7.2 %all-to-all-done.1 = bf16[8,16,512]{2,1,0:T(8,128)(2,1)S(1)} async-done(((bf16[8,16,512]{2,1,0:T(8,128)(2,1)}), bf16[8,16,512]{2,1,0:T(8,128)(2,1)S(1)}, u32[]{:S(2)}, u32[]{:S(2)}) %all-to-all-start.1) | async-done | bytes 131104 | tf_op jit(solution)/shard_map/all_to_all | solution.py:155
  169.6 0.2 fusion.15
  169.8 52.6 %reduce-scatter.8.cloned.1.call-done = bf16[32,512]{1,0:T(8,128)(2,1)} async-done(((bf16[256,512]{1,0:T(8,128)(2,1)}), bf16[32,512]{1,0:T(8,128)(2,1)}) %reduce-scatter.8.cloned.1.call-update) | async-done | bytes 32784 | tf_op jit(solution)/shard_map/reduce_scatter | solution.py:121
  222.4 0.9 multiply_reduce_fusion.1
  223.3 5.7 %psum.63 = f32[32]{0:T(128)S(1)} all-reduce(f32[32]{0:T(128)S(1)} %multiply_reduce_fusion.1), channel_id=1, replica_groups=mesh['ep'=8,'tp'=4] {'tp'}, use_global_device_ids=true, to_apply=%region_22.23 | all-reduce | flops 32 | bytes 256 | tf_op jit(solution)/shard_map/psum | solution.py:169
  229.0 1.5 add_convert_fusion
  (33 shorter events, 0.3 us)
Async XLA Ops:
  7.2 18.1 %copy-start = (bf16[256,2048]{1,0:T(8,128)(2,1)S(1)}, bf16[256,2048]{1,0:T(8,128)(2,1)}, u32[]{:S(2)}) copy-start(bf16[256,2048]{1,0:T(8,128)(2,1)} %param.31) | copy-start | bytes 3145732
  7.2 11.2 %copy-start.2 = (bf16[32,2048]{1,0:T(8,128)(2,1)S(1)}, bf16[32,2048]{1,0:T(8,128)(2,1)}, u32[]{:S(2)}) copy-start(bf16[32,2048]{1,0:T(8,128)(2,1)} %param.22) | copy-start | bytes 393220
  7.2 10.3 %copy-start.6 = (f32[32,2,128]{2,1,0:T(2,128)S(1)}, f32[32,2,128]{2,1,0:T(2,128)}, u32[]{:S(2)}) copy-start(f32[32,2,128]{2,1,0:T(2,128)} %param.33) | copy-start | bytes 98308
  7.2 11.2 %copy-start.3 = (bf16[2048,256]{1,0:T(8,128)(2,1)S(1)}, bf16[2048,256]{1,0:T(8,128)(2,1)}, u32[]{:S(2)}) copy-start(bf16[2048,256]{1,0:T(8,128)(2,1)} %param.27) | copy-start | bytes 3145732
  7.2 41.5 %reduce-scatter.4.cloned.1.call-start = ((), (), s32[]{:S(2)}) async-start(), calls=%async_computation.5 | async-start | bytes 163840 | tf_op jit(solution)/shard_map/reduce_scatter | solution.py:83
  13.9 8.5 %copy-start.7 = (f32[32,2]{0,1:T(2,128)}, f32[32,2]{0,1:T(2,128)S(1)}, u32[]{:S(2)}) copy-start(f32[32,2]{0,1:T(2,128)S(1)} %get-tuple-element.22) | copy-start | bytes 772
  22.4 2.0 copy-start.1
  24.5 1.7 copy-start.9
  24.5 63.0 %copy-start.4 = (bf16[512,704]{0,1:T(8,128)(2,1)S(1)}, bf16[512,704]{0,1:T(8,128)(2,1)}, u32[]{:S(2)}) copy-start(bf16[512,704]{0,1:T(8,128)(2,1)} %param.41) | copy-start | bytes 2162692
  24.5 63.4 %copy-start.5 = (bf16[512,704]{0,1:T(8,128)(2,1)S(1)}, bf16[512,704]{0,1:T(8,128)(2,1)}, u32[]{:S(2)}) copy-start(bf16[512,704]{0,1:T(8,128)(2,1)} %param.40) | copy-start | bytes 2162692
  89.2 12.6 %all-to-all-start = ((bf16[8,16,512]{2,1,0:T(8,128)(2,1)}), bf16[8,16,512]{2,1,0:T(8,128)(2,1)S(1)}, u32[]{:S(2)}, u32[]{:S(2)}) async-start(bf16[8,16,512]{2,1,0:T(8,128)(2,1)} %bitcast.6), calls=%async_computation.1 | async-start | bytes 262144 | tf_op jit(solution)/shard_map/all_to_all | solution.py:145
  94.5 38.1 %all-reduce.3.cloned.1.call-start = ((), (), s32[]{:S(2)}) async-start(), calls=%async_computation.7 | async-start | bytes 1441792 | tf_op jit(solution)/shard_map/psum | solution.py:118
  95.5 61.3 %reduce-scatter.6.cloned.1.call-start = ((), (), s32[]{:S(2)}) async-start(), calls=%async_computation.6 | async-start | bytes 655360 | tf_op jit(solution)/shard_map/reduce_scatter | solution.py:152
  113.8 19.9 %copy-start.10 = (bf16[704,512]{1,0:T(8,128)(2,1)S(1)}, bf16[704,512]{1,0:T(8,128)(2,1)}, u32[]{:S(2)}) copy-start(bf16[704,512]{1,0:T(8,128)(2,1)} %param.42) | copy-start | bytes 2162692
  119.3 43.0 %copy-start.8 = (f32[32,2]{0,1:T(2,128)S(1)}, f32[32,2]{0,1:T(2,128)}, u32[]{:S(2)}) copy-start(f32[32,2]{0,1:T(2,128)} %param.36) | copy-start | bytes 772
  119.3 103.0 %reduce-scatter.8.cloned.1.call-start = ((), (), s32[]{:S(2)}) async-start(), calls=%async_computation.8 | async-start | bytes 294912 | tf_op jit(solution)/shard_map/reduce_scatter | solution.py:121
  156.7 12.9 %all-to-all-start.1 = ((bf16[8,16,512]{2,1,0:T(8,128)(2,1)}), bf16[8,16,512]{2,1,0:T(8,128)(2,1)S(1)}, u32[]{:S(2)}, u32[]{:S(2)}) async-start(bf16[8,16,512]{2,1,0:T(8,128)(2,1)} %bitcast.62), calls=%async_computation.3 | async-start | bytes 262144 | tf_op jit(solution)/shard_map/all_to_all | solution.py:155
Sparse Core Ops, SparseCore 0:
  26.3 22.3 reduce-scatter.3
  97.7 34.8 all-reduce.2
  135.0 21.6 reduce-scatter.5
  159.9 62.4 reduce-scatter.7
where the time goes:
time: 238 us; the launch traced here: 237 us
  waiting for transfers between devices  121 us (51%)
  blocking collectives  51.8 us (22%)
  matrix products  20.2 us (8%)
  between operations  14.1 us (6%)
  other arithmetic  13.3 us (6%)
  starting transfers between devices  11 us (5%)
  local copies, waits for them, and re-layouts  5.31 us (2%)
    reduce_scatter x1, waiting for transfers between devices, local(): lax.psum_scatter(jnp.dot(dense_hidden, dense_down, preferred_element_type...  52.6 us
    all_gather x1, blocking collectives, local(): rows_in = lax.all_gather(normed, 'ep', axis=0, tiled=True)  31.2 us
    reduce_scatter x1, waiting for transfers between devices, local(): lax.psum_scatter(partial_out.astype(jnp.bfloat16), 'tp', scatter_dimensio...  21.8 us
    reduce_scatter x1, waiting for transfers between devices, local(): lax.psum_scatter(branch_terms.astype(jnp.bfloat16), 'tp', scatter_dimensi...  20.2 us
    psum x1, waiting for transfers between devices, local(): lax.psum(dense_pre.astype(jnp.bfloat16), 'tp').astype(jnp.float32)  13.2 us
    all_gather x1, blocking collectives, local(): full_rows = lax.all_gather(arrived, 'tp', axis=2, tiled=True)  9.21 us
    all_to_all x1, waiting for transfers between devices, local(): lax.all_to_all(summed_out.reshape(arrived.shape), 'ep', split_axis=0, con...  7.21 us
    all_to_all x1, waiting for transfers between devices, local(): lax.all_to_all(outgoing, 'ep', split_axis=0, concat_axis=0, tiled=True)  6.31 us
  transfers between devices with their start and end apart: 6, of which 6 were waited for; matrix products, arithmetic and copies ran while one was open for 6% of the time, Pallas kernels for 0%

commit v1 on v0

v1 whole, which is shorter than its diff:
```python
import jax
import jax.numpy as jnp
from jax import lax
from jax.sharding import PartitionSpec as P

EPS = 1e-06
F32 = jnp.float32
BF16 = jnp.bfloat16


def settle(values):
    return lax.optimization_barrier(values.astype(BF16)).astype(F32)


def dot(left, right):
    return jnp.dot(left, right, preferred_element_type=F32)


def swap(values, axis, step):
    count = lax.axis_size(axis)
    return lax.ppermute(values, axis, [(i, i ^ step) for i in range(count)])


def gather_own_first(values, axis):
    return [values] + [swap(values, axis, j) for j in range(1, lax.axis_size(axis))]


def in_order(pieces, place):
    stacked = jnp.stack(pieces)
    return [
        lax.dynamic_index_in_dim(stacked, place ^ j, 0, keepdims=False) for j in range(len(pieces))
    ]


def add_pieces(pieces):
    total = pieces[0].astype(F32)
    for piece in pieces[1:]:
        total = total + piece.astype(F32)
    return total


def steps_of(count):
    steps, step = [], count // 2
    while step:
        steps.append(step)
        step //= 2
    return steps


def three_parts(values):
    high = lax.reduce_precision(values, 8, 7)
    rest = values - high
    middle = lax.reduce_precision(rest, 8, 7)
    return [high, middle, rest - middle]


def local(
    hidden,
    norm_gains,
    w_query,
    w_key,
    w_value,
    w_outgate,
    w_input_gate,
    w_forget_gate,
    forget_bias,
    w_mix_out,
    state_matrix,
    state_norm,
    state_max,
    routes,
    route_scores,
    expert_gate,
    expert_up,
    expert_down,
    dense_gate,
    dense_up,
    dense_down,
    dense_mix,
):
    tp_count = lax.axis_size("tp")
    ep_count = lax.axis_size("ep")
    tp_place = lax.axis_index("tp")
    ep_place = lax.axis_index("ep")
    seq_local, width = hidden.shape
    heads_local = state_matrix.shape[1]
    head_width = state_matrix.shape[2]
    part_width = width // tp_count
    feature_first = tp_place * part_width
    route_width = routes.shape[1]
    capacity = 2 * seq_local * route_width // ep_count

    flat_expert = routes.reshape(-1)
    pair = jnp.arange(flat_expert.shape[0], dtype=jnp.int32)
    ranks = jnp.sum(
        (
            (flat_expert[:, None] == flat_expert[None, :]) & (pair[None, :] < pair[:, None])
        ).astype(jnp.int32),
        axis=1,
    ).reshape(routes.shape)
    share = route_scores / jnp.sum(route_scores, axis=-1, keepdims=True)

    start_f = hidden.astype(F32)
    normed_in = (
        start_f
        * lax.rsqrt(jnp.mean(start_f * start_f, axis=-1, keepdims=True) + EPS)
        * norm_gains[0]
    ).astype(BF16)
    query_f = dot(normed_in, w_query)
    key_f = dot(normed_in, w_key)
    value_f = dot(normed_in, w_value)
    gate_f = dot(normed_in, w_outgate)
    head_first = tp_place * heads_local
    input_weight = lax.dynamic_slice_in_dim(w_input_gate, head_first, heads_local, 1)
    forget_weight = lax.dynamic_slice_in_dim(w_forget_gate, head_first, heads_local, 1)
    forget_local = lax.dynamic_slice_in_dim(forget_bias, head_first, heads_local, 0)
    in_gate = dot(normed_in, input_weight)
    log_forget = jax.nn.log_sigmoid(dot(normed_in, forget_weight) + forget_local)
    query = settle(query_f).reshape(seq_local, heads_local, head_width)
    keys = settle(key_f).reshape(seq_local, heads_local, head_width) * head_width ** (-0.5)
    values = settle(value_f).reshape(seq_local, heads_local, head_width)
    carried = log_forget + state_max
    new_max = jnp.maximum(carried, in_gate)
    keep = jnp.exp(carried - new_max)
    write = jnp.exp(in_gate - new_max)
    written = write[:, :, None] * keys
    new_matrix = (
        keep[:, :, None, None] * state_matrix + written[:, :, :, None] * values[:, :, None, :]
    )
    new_norm = keep[:, :, None] * state_norm + written
    numer = jnp.einsum("shd,shdv->shv", query, new_matrix)
    denom = jnp.einsum("shd,shd->sh", query, new_norm)
    read = numer / jnp.maximum(jnp.abs(denom), jnp.exp(-new_max))[:, :, None]
    mixed = (
        jax.nn.sigmoid(settle(gate_f)) * read.reshape(seq_local, heads_local * head_width)
    ).astype(BF16)
    branch_terms = lax.optimization_barrier(dot(mixed, w_mix_out).astype(BF16))

    branch = settle(add_pieces(gather_own_first(branch_terms, "tp")))
    branch_scale = lax.rsqrt(jnp.mean(branch * branch, axis=-1, keepdims=True) + EPS)
    residual_f = start_f + norm_gains[1] * branch * branch_scale
    scale_two = lax.rsqrt(jnp.mean(residual_f * residual_f, axis=-1, keepdims=True) + EPS)
    gained = residual_f * norm_gains[2]
    mix_gate = jax.nn.sigmoid(
        scale_two * jnp.sum(gained * dense_mix, axis=-1, keepdims=True)
    )
    residual_part = settle(lax.dynamic_slice_in_dim(residual_f, feature_first, part_width, 1))
    normed = (
        lax.dynamic_slice_in_dim(gained, feature_first, part_width, 1) * scale_two
    ).astype(BF16)

    numbers = [routes.astype(F32), ranks.astype(F32)] + three_parts(share) + three_parts(mix_gate)
    notes = jnp.concatenate(numbers, axis=1).astype(BF16)
    notes = jnp.pad(notes, ((0, 0), (0, 128 - notes.shape[1])))
    blocks = jnp.concatenate([normed, notes], axis=1)[None]
    ep_steps = steps_of(ep_count)
    for step in ep_steps:
        blocks = jnp.concatenate([blocks, swap(blocks, "ep", step)], axis=0)
    rows_all = ep_count * seq_local
    rows_in = blocks[:, :, :part_width].reshape(rows_all, part_width)
    notes_in = blocks[:, :, part_width:].reshape(rows_all, 128).astype(F32)
    route_in = notes_in[:, :route_width]
    rank_in = notes_in[:, route_width : 2 * route_width]
    shares = [
        notes_in[:, route_width * k : route_width * (k + 1)] for k in range(2, 5)
    ]
    share_in = shares[0] + shares[1] + shares[2]
    mix_at = 5 * route_width
    mix_in = (
        notes_in[:, mix_at : mix_at + 1]
        + notes_in[:, mix_at + 1 : mix_at + 2]
        + notes_in[:, mix_at + 2 : mix_at + 3]
    )
    here = (route_in == ep_place.astype(F32)).astype(F32)
    block_first = (jnp.arange(rows_all, dtype=jnp.int32) // seq_local * capacity).astype(F32)
    named = jnp.sum(here, axis=1)
    slot_in = jnp.where(
        named > 0, jnp.sum(here * rank_in, axis=1) + block_first, -1.0
    )
    weight_in = jnp.sum(here * share_in, axis=1, keepdims=True)
    slots = ep_count * capacity
    placing = (
        jnp.arange(slots, dtype=jnp.int32).astype(F32)[:, None] == slot_in[None, :]
    ).astype(BF16)

    expert_rows = dot(placing, rows_in).astype(BF16)
    flat_rows = jnp.concatenate(
        in_order(gather_own_first(expert_rows, "tp"), tp_place), axis=1
    )

    dense_rows = rows_all // tp_count
    dense_pre = jnp.concatenate([dot(rows_in, dense_gate), dot(rows_in, dense_up)], axis=1)
    dense_pre = dense_pre.astype(BF16).reshape(tp_count, dense_rows, -1)
    pre_pieces = [
        lax.dynamic_index_in_dim(dense_pre, tp_place ^ j, 0, keepdims=False)
        for j in range(tp_count)
    ]
    pre_sum = add_pieces(
        [pre_pieces[0]] + [swap(pre_pieces[j], "tp", j) for j in range(1, tp_count)]
    )
    pre_gate, pre_up = jnp.split(pre_sum, 2, axis=1)
    dense_own = (jax.nn.silu(pre_gate) * pre_up).astype(BF16)
    dense_hidden = jnp.concatenate(
        in_order(gather_own_first(dense_own, "tp"), tp_place), axis=0
    )

    gate_pre = dot(flat_rows, expert_gate[0])
    up_pre = dot(flat_rows, expert_up[0])
    hidden_units = (jax.nn.silu(gate_pre) * up_pre).astype(BF16)
    partial_out = lax.optimization_barrier(dot(hidden_units, expert_down[0]).astype(BF16))
    out_pieces = [
        lax.dynamic_slice_in_dim(partial_out, (tp_place ^ j) * part_width, part_width, 1)
        for j in range(tp_count)
    ]
    expert_out = add_pieces(
        [out_pieces[0]] + [swap(out_pieces[j], "tp", j) for j in range(1, tp_count)]
    ).astype(BF16)

    picked = lax.dot_general(
        placing, expert_out, (((0,), (0,)), ((), ())), preferred_element_type=F32
    )
    given = weight_in * picked + mix_in * dot(dense_hidden, dense_down)
    given = given.reshape(ep_count, seq_local, part_width)
    for step in reversed(ep_steps):
        half = given.shape[0] // 2
        given = given[:half] + swap(given[half:].astype(BF16), "ep", step).astype(F32)
    ffn = given[0]
    ffn_sq = jnp.broadcast_to(jnp.sum(ffn * ffn, axis=-1, keepdims=True), (seq_local, 128))
    ffn_sq = add_pieces(gather_own_first(ffn_sq, "tp"))[:, :1]
    gain_last = lax.dynamic_slice_in_dim(norm_gains[3], feature_first, part_width, 0)
    new_hidden = (residual_part + gain_last * ffn * lax.rsqrt(ffn_sq / width + EPS)).astype(BF16)
    return (new_hidden, new_matrix, new_norm, new_max)


def solution(mesh):
    placed = (
        P("ep", None),
        P(),
        P(None, "tp"),
        P(None, "tp"),
        P(None, "tp"),
        P(None, "tp"),
        P(),
        P(),
        P(),
        P("tp", None),
        P("ep", "tp", None, None),
        P("ep", "tp", None),
        P("ep", "tp"),
        P("ep", None),
        P("ep", None),
        P("ep", None, "tp"),
        P("ep", None, "tp"),
        P("ep", "tp", None),
        P("tp", "ep"),
        P("tp", "ep"),
        P("ep", "tp"),
        P(),
    )
    return jax.shard_map(
        local,
        mesh=mesh,
        in_specs=placed,
        out_specs=(P("ep", "tp"), P("ep", "tp", None, None), P("ep", "tp", None), P("ep", "tp")),
        check_vma=False,
    )
```

time: 238 us -> 99.9 us (0.42)
  waiting for transfers between devices: 121 us -> 34.9 us
  blocking collectives: 51.8 us -> 0 us
  starting transfers between devices: 11 us -> 27.7 us
  between operations: 14.1 us -> 1.12 us
    reduce_scatter x3 -> x0, waiting for transfers between devices: 94.7 us -> none  [the longest x1 52.6 us: local(): lax.psum_scatter(jnp.dot(dense_hidden, dense_down, preferred_element_type...]
    all_gather x2 -> x0, blocking collectives: 40.4 us -> none  [the longest x1 31.2 us: local(): rows_in = lax.all_gather(normed, 'ep', axis=0, tiled=True)]
    ppermute x0 -> x24, waiting for transfers between devices: none -> 34.9 us  [swap(): return lax.ppermute(values, axis, [(i, i ^ step) for i in range(count)])]
    ppermute x0 -> x24, starting transfers between devices: none -> 27.7 us  [swap(): return lax.ppermute(values, axis, [(i, i ^ step) for i in range(count)])]
    all_to_all x2 -> x0, waiting for transfers between devices: 13.5 us -> none  [the longest x1 7.21 us: local(): lax.all_to_all(summed_out.reshape(arrived.shape), 'ep', split_axis=0, con...]
    psum x1 -> x0, waiting for transfers between devices: 13.2 us -> none  [local(): lax.psum(dense_pre.astype(jnp.bfloat16), 'tp').astype(jnp.float32)]
    psum x2 -> x0, blocking collectives: 11.4 us -> none  [the longest x1 5.77 us: local(): lax.psum((jnp.sum(branch * branch, axis=-1), jnp.sum(start_part * start_p...]
    all_to_all x2 -> x0, starting transfers between devices: 10.8 us -> none  [the longest x1 5.52 us: local(): lax.all_to_all(summed_out.reshape(arrived.shape), 'ep', split_axis=0, con...]
  transfers between devices with their start and end apart: 6 -> 24, of which waited for: 6 -> 14; matrix products, arithmetic and copies ran while one was open for 6% -> 14% of each run, Pallas kernels for 0% -> 0%
where the time goes in v1:
time: 99.9 us; the launch traced here: 99.5 us
  waiting for transfers between devices  34.9 us (35%)
  starting transfers between devices  27.7 us (28%)
  matrix products  18.9 us (19%)
  other arithmetic  11.4 us (11%)
  local copies, waits for them, and re-layouts  5.34 us (5%)
  between operations  1.12 us (1%)
    ppermute x24, waiting for transfers between devices, swap(): return lax.ppermute(values, axis, [(i, i ^ step) for i in range(count)])  34.9 us
    ppermute x24, starting transfers between devices, swap(): return lax.ppermute(values, axis, [(i, i ^ step) for i in range(count)])  27.7 us
    dot_general x13, matrix products, dot(): return jnp.dot(left, right, preferred_element_type=F32)  18 us
    add x1, other arithmetic, local(): keep[:, :, None, None] * state_matrix  3.7 us
    unnamed x33, local copies, waits for them, and re-layouts  2.51 us
  transfers between devices with their start and end apart: 24, of which 14 were waited for; matrix products, arithmetic and copies ran while one was open for 14% of the time, Pallas kernels for 0%

profile of v1, /device:TPU:0, one launch (start us, length us, event | category | flops | bytes accessed | tf_op | source)
XLA Modules:
  0.0 99.5 jit_solution(10813284372128623599)
XLA Ops:
  0.7 1.0 fusion.98
  1.7 1.0 %fusion.37 = f32[32]{0:T(128)S(1)} fusion(bf16[32,2048]{1,0:T(8,128)(2,1)} %param.22), kind=kLoop, calls=%fused_computation.58 | loop fusion | flops 196576 | bytes 131200 | tf_op jit(solution)/shard_map/reduce_sum | solution.py:106
  2.7 1.6 %convolution_convert_fusion.6 = bf16[32,256]{1,0:T(8,128)(2,1)S(1)} fusion(bf16[2048,256]{1,0:T(8,128)(2,1)} %param.24, bf16[32,2048]{1,0:T(8,128)(2,1)} %param.22, f32[2048]{0:T(1024)S(1)} %bitcast.112, f32[32]{0:T(128)S(1)} %add_rsqrt_fusion.2), kind=kOutput, calls=%fused_computation.19 | convolution fusion | flops 33824768 | bytes 1204352 | tf_op jit(solution)/shard_map/dot_general | solution.py:16
  4.4 1.6 %convolution_convert_fusion.4 = bf16[32,256]{1,0:T(8,128)(2,1)S(1)} fusion(bf16[2048,256]{1,0:T(8,128)(2,1)} %param.26, bf16[32,2048]{1,0:T(8,128)(2,1)} %param.22, f32[2048]{0:T(1024)S(1)} %bitcast.113, f32[32]{0:T(128)S(1)} %add_rsqrt_fusion.2), kind=kOutput, calls=%fused_computation.17 | convolution fusion | flops 33824768 | bytes 1204352 | tf_op jit(solution)/shard_map/dot_general | solution.py:16
  6.1 1.1 %fusion.69 = f32[32,2]{0,1:T(2,128)S(1)} fusion(bf16[2048,8]{0,1:T(8,128)(2,1)} %param.28, s32[]{:T(128)S(6)} %select_n.65, bf16[32,2048]{1,0:T(8,128)(2,1)} %param.22, f32[2048]{0:T(1024)S(1)} %bitcast.114, f32[32]{0:T(128)S(1)} %add_rsqrt_fusion.2), kind=kOutput, calls=%fused_computation.132 | convolution fusion | flops 524288 | bytes 147844 | tf_op jit(solution)/shard_map/dot_general | solution.py:16
  7.2 0.7 dynamic_slice.70
  7.9 1.2 %subtract_exponential_fusion = (f32[32,2]{0,1:T(2,128)S(1)}, f32[32,2]{0,1:T(2,128)S(1)}) fusion(f32[32,2]{0,1:T(2,128)S(1)} %fusion.69, f32[32,2]{0,1:T(2,128)} %param.34, f32[2]{0:T(128)S(1)} %dynamic_slice.70, bf16[2048,8]{0,1:T(8,128)(2,1)} %param.29, s32[]{:T(128)S(6)} %select_n.65, bf16[32,2048]{1,0:T(8,128)(2,1)} %param.22, f32[2048]{0:T(1024)S(1)} %bitcast.115, ...), kind=kOutput, calls=%fused_computation.162 | convolution fusion | flops 525056 | bytes 149388 | tf_op jit(solution)/shard_map/dot_general | solution.py:16
  9.2 1.6 %convolution_convert_fusion.5 = bf16[32,256]{1,0:T(8,128)(2,1)S(1)} fusion(bf16[2048,256]{1,0:T(8,128)(2,1)} %param.25, bf16[32,2048]{1,0:T(8,128)(2,1)} %param.22, f32[2048]{0:T(1024)S(1)} %bitcast.116, f32[32]{0:T(128)S(1)} %add_rsqrt_fusion.2), kind=kOutput, calls=%fused_computation.18 | convolution fusion | flops 33824768 | bytes 1204352 | tf_op jit(solution)/shard_map/dot_general | solution.py:16
  11.0 0.8 fusion.65
  11.9 0.3 convolution_convert_fusion.7
  12.2 3.7 %multiply_add_fusion = f32[32,2,128,128]{3,2,1,0:T(8,128)S(1)} fusion(f32[32,2,128,128]{3,2,1,0:T(8,128)} %param.32, f32[32,2,128]{2,1,0:T(2,128)S(1)} %reshape.190, f32[32,2,128]{2,1,0:T(2,128)S(1)} %get-tuple-element.17, f32[32,2]{1,0:T(8,128)S(1)} %copy.65), kind=kLoop, calls=%fused_computation | loop fusion | flops 3145728 | bytes 8454400 | tf_op jit(solution)/shard_map/add | solution.py:128
  16.0 2.0 %copy-done.1 = f32[32,2,128,128]{3,2,1,0:T(8,128)} copy-done((f32[32,2,128,128]{3,2,1,0:T(8,128)}, f32[32,2,128,128]{3,2,1,0:T(8,128)S(1)}, u32[]{:S(2)}) %copy-start.1) | copy-done | bytes 4194328
  18.0 0.7 fusion.99
  18.8 0.3 convolution_convert_fusion
  19.0 2.5 %collective-permute-start.2 = (bf16[32,2048]{1,0:T(8,128)(2,1)S(1)}, bf16[32,2048]{1,0:T(8,128)(2,1)S(1)}, u32[]{:S(2)}, u32[]{:S(2)}) collective-permute-start(bf16[32,2048]{1,0:T(8,128)(2,1)S(1)} %convolution_convert_fusion), channel_id=1, source_target_pairs={{0,3},{1,2},{2,1},{3,0},{4,7},{5,6},{6,5},{7,4},{8,11},{9,10},{10,... | collective-permute-start | bytes 393224 | tf_op jit(solution)/shard_map/ppermute | solution.py:21
  21.5 0.6 collective-permute-start.1
  22.4 0.2 convert_reduce_fusion.1
  22.8 2.5 %collective-permute-done.2 = bf16[32,2048]{1,0:T(8,128)(2,1)S(1)} collective-permute-done((bf16[32,2048]{1,0:T(8,128)(2,1)S(1)}, bf16[32,2048]{1,0:T(8,128)(2,1)S(1)}, u32[]{:S(2)}, u32[]{:S(2)}) %collective-permute-start.2) | collective-permute-done | bytes 131104 | tf_op jit(solution)/shard_map/ppermute | solution.py:21
  25.4 3.0 %collective-permute-done.1 = bf16[32,2048]{1,0:T(8,128)(2,1)S(1)} collective-permute-done((bf16[32,2048]{1,0:T(8,128)(2,1)S(1)}, bf16[32,2048]{1,0:T(8,128)(2,1)S(1)}, u32[]{:S(2)}, u32[]{:S(2)}) %collective-permute-start.1) | collective-permute-done | bytes 131104 | tf_op jit(solution)/shard_map/ppermute | solution.py:21
  28.4 0.1 fusion.36
  28.6 0.2 multiply_reduce_fusion.1
  28.8 0.1 multiply_reduce_fusion
  29.3 3.5 %collective-permute-start.3 = (bf16[1,32,640]{2,1,0:T(8,128)(2,1)S(1)}, bf16[1,32,640]{2,1,0:T(8,128)(2,1)S(1)}, u32[]{:S(2)}, u32[]{:S(2)}) collective-permute-start(bf16[1,32,640]{2,1,0:T(8,128)(2,1)S(1)} %fusion.63), channel_id=1, source_target_pairs={{0,16},{4,20},{8,24},{12,28},{16,0},{20,4},{24,8},{28,12},{1,17},{... | collective-permute-start | bytes 122888 | tf_op jit(solution)/shard_map/ppermute | solution.py:21
  32.7 2.0 %collective-permute-done.3 = bf16[1,32,640]{2,1,0:T(8,128)(2,1)S(1)} collective-permute-done((bf16[1,32,640]{2,1,0:T(8,128)(2,1)S(1)}, bf16[1,32,640]{2,1,0:T(8,128)(2,1)S(1)}, u32[]{:S(2)}, u32[]{:S(2)}) %collective-permute-start.3) | collective-permute-done | bytes 40992 | tf_op jit(solution)/shard_map/ppermute | solution.py:21
  34.7 2.0 %collective-permute-start.4 = (bf16[2,32,640]{2,1,0:T(8,128)(2,1)S(1)}, bf16[2,32,640]{2,1,0:T(8,128)(2,1)S(1)}, u32[]{:S(2)}, u32[]{:S(2)}) collective-permute-start(bf16[2,32,640]{2,1,0:T(8,128)(2,1)S(1)} %pad_maximum_fusion.10), channel_id=1, source_target_pairs={{0,8},{4,12},{8,0},{12,4},{16,24},{20,28},{24,16},{28,20},{1,9},{5... | collective-permute-start | bytes 245768 | tf_op jit(solution)/shard_map/ppermute | solution.py:21
  36.7 2.5 %collective-permute-done.4 = bf16[2,32,640]{2,1,0:T(8,128)(2,1)S(1)} collective-permute-done((bf16[2,32,640]{2,1,0:T(8,128)(2,1)S(1)}, bf16[2,32,640]{2,1,0:T(8,128)(2,1)S(1)}, u32[]{:S(2)}, u32[]{:S(2)}) %collective-permute-start.4) | collective-permute-done | bytes 81952 | tf_op jit(solution)/shard_map/ppermute | solution.py:21
  39.3 2.4 %collective-permute-start.5 = (bf16[4,32,640]{2,1,0:T(8,128)(2,1)S(1)}, bf16[4,32,640]{2,1,0:T(8,128)(2,1)S(1)}, u32[]{:S(2)}, u32[]{:S(2)}) collective-permute-start(bf16[4,32,640]{2,1,0:T(8,128)(2,1)S(1)} %pad_maximum_fusion.6), channel_id=1, source_target_pairs={{0,4},{4,0},{8,12},{12,8},{16,20},{20,16},{24,28},{28,24},{1,5},{5... | collective-permute-start | bytes 491528 | tf_op jit(solution)/shard_map/ppermute | solution.py:21
  41.6 3.3 %collective-permute-done.5 = bf16[4,32,640]{2,1,0:T(8,128)(2,1)S(1)} collective-permute-done((bf16[4,32,640]{2,1,0:T(8,128)(2,1)S(1)}, bf16[4,32,640]{2,1,0:T(8,128)(2,1)S(1)}, u32[]{:S(2)}, u32[]{:S(2)}) %collective-permute-start.5) | collective-permute-done | bytes 163872 | tf_op jit(solution)/shard_map/ppermute | solution.py:21
  44.9 0.1 fusion.97
  45.1 0.3 fusion.52
  45.5 0.9 convolution_convert_fusion.3
  46.3 2.0 %collective-permute-start.7 = (bf16[128,512]{1,0:T(8,128)(2,1)}, bf16[128,512]{1,0:T(8,128)(2,1)}, u32[]{:S(2)}, u32[]{:S(2)}) collective-permute-start(bf16[128,512]{1,0:T(8,128)(2,1)} %convolution_convert_fusion.3), channel_id=1, source_target_pairs={{0,2},{1,3},{2,0},{3,1},{4,6},{5,7},{6,4},{7,5},{8,10},{9,11},{10,... | collective-permute-start | bytes 393224 | tf_op jit(solution)/shard_map/ppermute | solution.py:21
  48.4 0.4 convolution_convert_fusion.2
  48.9 0.4 convolution_convert_fusion.1
  49.3 1.0 fusion.47
  50.2 1.4 %collective-permute-start.14 = (bf16[64,1408]{1,0:T(8,128)(2,1)}, bf16[64,1408]{1,0:T(8,128)(2,1)}, u32[]{:S(2)}, u32[]{:S(2)}) collective-permute-start(bf16[64,1408]{1,0:T(8,128)(2,1)} %get-tuple-element.22), channel_id=1, source_target_pairs={{0,3},{1,2},{2,1},{3,0},{4,7},{5,6},{6,5},{7,4},{8,11},{9,10},{10,... | collective-permute-start | bytes 540680 | tf_op jit(solution)/shard_map/ppermute | solution.py:21
  51.6 0.7 collective-permute-start.13
  52.5 0.3 collective-permute-start.12
  52.8 3.0 %collective-permute-done.7 = bf16[128,512]{1,0:T(8,128)(2,1)} collective-permute-done((bf16[128,512]{1,0:T(8,128)(2,1)}, bf16[128,512]{1,0:T(8,128)(2,1)}, u32[]{:S(2)}, u32[]{:S(2)}) %collective-permute-start.7) | collective-permute-done | bytes 131104 | tf_op jit(solution)/shard_map/ppermute | solution.py:21
  55.8 1.2 %pad_maximum_fusion = bf16[4,128,512]{2,1,0:T(8,128)(2,1)S(1)} fusion(bf16[1,128,512]{2,1,0:T(8,128)(2,1)} %bitcast.14, bf16[1,128,512]{2,1,0:T(8,128)(2,1)} %bitcast.13, bf16[1,128,512]{2,1,0:T(8,128)(2,1)} %bitcast.12, bf16[1,128,512]{2,1,0:T(8,128)(2,1)} %bitcast.11), kind=kLoop, calls=%fused_computation.33 | loop fusion | flops 786432 | bytes 1048576 | tf_op jit(solution)/shard_map/stack | solution.py:29
  57.0 3.5 %fusion.4 = f32[128,896]{1,0:T(8,128)} fusion(bf16[1,2048,896]{2,1,0:T(8,128)(2,1)} %param.37, bf16[128,512]{1,0:T(8,128)(2,1)S(1)} %get-tuple-element.27, bf16[128,512]{1,0:T(8,128)(2,1)S(1)} %get-tuple-element.28, bf16[128,512]{1,0:T(8,128)(2,1)S(1)} %get-tuple-element.29, bf16[128,512]{1,0:T(8,128)(2,1)S(1)} %get-tuple-element.26), kind=kOutput, calls=%fused_computation.5 | convolution fusion | flops 471859200 | bytes 4653056 | tf_op jit(solution)/shard_map/dot_general | solution.py:16
  60.6 4.6 %fusion.6 = bf16[128,2048]{1,0:T(8,128)(2,1)S(1)} fusion(bf16[1,896,2048]{2,1,0:T(8,128)(2,1)} %param.39, bf16[1,2048,896]{2,1,0:T(8,128)(2,1)} %param.38, f32[128,896]{1,0:T(8,128)} %fusion.4, bf16[128,512]{1,0:T(8,128)(2,1)S(1)} %get-tuple-element.27, bf16[128,512]{1,0:T(8,128)(2,1)S(1)} %get-tuple-element.28, bf16[128,512]{1,0:T(8,128)(2,1)S(1)} %get-tuple-element.29, ...), kind=kOutput, calls=%fused_computation.7 | convolution fusion | flops 942571520 | bytes 8847360 | tf_op jit(solution)/shard_map/dot_general | solution.py:16
  65.3 0.6 collective-permute-start.10
  66.0 1.1 %fusion.34 = f32[64,1408]{1,0:T(8,128)S(1)} fusion(bf16[64,1408]{1,0:T(8,128)(2,1)} %collective-permute-done.14, bf16[64,1408]{1,0:T(8,128)(2,1)} %collective-permute-done.13, bf16[64,1408]{1,0:T(8,128)(2,1)S(1)} %collective-permute-done.12, s32[]{:T(128)S(6)} %select_n.70, bf16[4,64,704]{2,1,0:T(8,128)(2,1)S(1)} %convolution_convert_fusion.2, ...), kind=kLoop, calls=%fused_computation.53 | loop fusion | flops 991232 | bytes 1622020 | tf_op jit(solution)/shard_map/add | solution.py:38
  67.1 0.1 fusion.41
  67.3 1.2 %collective-permute-start.17 = (bf16[64,704]{1,0:T(8,128)(2,1)S(1)}, bf16[64,704]{1,0:T(8,128)(2,1)S(1)}, u32[]{:S(2)}, u32[]{:S(2)}) collective-permute-start(bf16[64,704]{1,0:T(8,128)(2,1)S(1)} %fusion.41), channel_id=1, source_target_pairs={{0,3},{1,2},{2,1},{3,0},{4,7},{5,6},{6,5},{7,4},{8,11},{9,10},{10,... | collective-permute-start | bytes 270344 | tf_op jit(solution)/shard_map/ppermute | solution.py:21
  68.4 1.7 %collective-permute-start.16 = (bf16[64,704]{1,0:T(8,128)(2,1)S(1)}, bf16[64,704]{1,0:T(8,128)(2,1)S(1)}, u32[]{:S(2)}, u32[]{:S(2)}) collective-permute-start(bf16[64,704]{1,0:T(8,128)(2,1)S(1)} %fusion.41), channel_id=1, source_target_pairs={{0,2},{1,3},{2,0},{3,1},{4,6},{5,7},{6,4},{7,5},{8,10},{9,11},{10,... | collective-permute-start | bytes 270344 | tf_op jit(solution)/shard_map/ppermute | solution.py:21
  70.2 0.1 fusion.111
  70.3 5.7 %collective-permute-done.17 = bf16[64,704]{1,0:T(8,128)(2,1)S(1)} collective-permute-done((bf16[64,704]{1,0:T(8,128)(2,1)S(1)}, bf16[64,704]{1,0:T(8,128)(2,1)S(1)}, u32[]{:S(2)}, u32[]{:S(2)}) %collective-permute-start.17) | collective-permute-done | bytes 90144 | tf_op jit(solution)/shard_map/ppermute | solution.py:21
  76.0 0.5 collective-permute-done.16
  76.7 0.4 convolution_multiply_fusion
  77.1 0.3 collective-permute-done.9
  77.4 0.3 fusion.9
  77.8 2.9 %collective-permute-start.18 = (bf16[4,32,512]{2,1,0:T(8,128)(2,1)S(1)}, bf16[4,32,512]{2,1,0:T(8,128)(2,1)S(1)}, u32[]{:S(2)}, u32[]{:S(2)}) collective-permute-start(bf16[4,32,512]{2,1,0:T(8,128)(2,1)S(1)} %bitcast.120), channel_id=1, source_target_pairs={{0,4},{4,0},{8,12},{12,8},{16,20},{20,16},{24,28},{28,24},{1,5},{5... | collective-permute-start | bytes 393224 | tf_op jit(solution)/shard_map/ppermute | solution.py:21
  80.7 3.5 %collective-permute-done.18 = bf16[4,32,512]{2,1,0:T(8,128)(2,1)S(1)} collective-permute-done((bf16[4,32,512]{2,1,0:T(8,128)(2,1)S(1)}, bf16[4,32,512]{2,1,0:T(8,128)(2,1)S(1)}, u32[]{:S(2)}, u32[]{:S(2)}) %collective-permute-start.18) | collective-permute-done | bytes 131104 | tf_op jit(solution)/shard_map/ppermute | solution.py:21
  84.3 1.4 %collective-permute-start.19 = (bf16[2,32,512]{2,1,0:T(8,128)(2,1)S(1)}, bf16[2,32,512]{2,1,0:T(8,128)(2,1)S(1)}, u32[]{:S(2)}, u32[]{:S(2)}) collective-permute-start(bf16[2,32,512]{2,1,0:T(8,128)(2,1)S(1)} %slice.149), channel_id=1, source_target_pairs={{0,8},{4,12},{8,0},{12,4},{16,24},{20,28},{24,16},{28,20},{1,9},{5... | collective-permute-start | bytes 196616 | tf_op jit(solution)/shard_map/ppermute | solution.py:21
  85.7 2.9 %collective-permute-done.19 = bf16[2,32,512]{2,1,0:T(8,128)(2,1)S(1)} collective-permute-done((bf16[2,32,512]{2,1,0:T(8,128)(2,1)S(1)}, bf16[2,32,512]{2,1,0:T(8,128)(2,1)S(1)}, u32[]{:S(2)}, u32[]{:S(2)}) %collective-permute-start.19) | collective-permute-done | bytes 65568 | tf_op jit(solution)/shard_map/ppermute | solution.py:21
  88.6 2.5 %collective-permute-start.20 = (bf16[1,32,512]{2,1,0:T(8,128)(2,1)S(1)}, bf16[1,32,512]{2,1,0:T(8,128)(2,1)S(1)}, u32[]{:S(2)}, u32[]{:S(2)}) collective-permute-start(bf16[1,32,512]{2,1,0:T(8,128)(2,1)S(1)} %slice.150), channel_id=1, source_target_pairs={{0,16},{4,20},{8,24},{12,28},{16,0},{20,4},{24,8},{28,12},{1,17},{... | collective-permute-start | bytes 98312 | tf_op jit(solution)/shard_map/ppermute | solution.py:21
  91.1 2.4 %collective-permute-done.20 = bf16[1,32,512]{2,1,0:T(8,128)(2,1)S(1)} collective-permute-done((bf16[1,32,512]{2,1,0:T(8,128)(2,1)S(1)}, bf16[1,32,512]{2,1,0:T(8,128)(2,1)S(1)}, u32[]{:S(2)}, u32[]{:S(2)}) %collective-permute-start.20) | collective-permute-done | bytes 32800 | tf_op jit(solution)/shard_map/ppermute | solution.py:21
  93.5 0.1 multiply_reduce_fusion.2
  93.8 1.8 %collective-permute-start.21 = (f32[32,128]{0,1:T(8,128)S(1)}, f32[32,128]{0,1:T(8,128)S(1)}, u32[]{:S(2)}, u32[]{:S(2)}) collective-permute-start(f32[32,128]{0,1:T(8,128)S(1)} %broadcast_in_dim.9), channel_id=1, source_target_pairs={{0,1},{1,0},{2,3},{3,2},{4,5},{5,4},{6,7},{7,6},{8,9},{9,8},{10,11... | collective-permute-start | bytes 49160 | tf_op jit(solution)/shard_map/ppermute | solution.py:21
  95.6 1.9 %collective-permute-done.23 = f32[32,128]{0,1:T(8,128)S(1)} collective-permute-done((f32[32,128]{0,1:T(8,128)S(1)}, f32[32,128]{0,1:T(8,128)S(1)}, u32[]{:S(2)}, u32[]{:S(2)}) %collective-permute-start.23) | collective-permute-done | bytes 16416 | tf_op jit(solution)/shard_map/ppermute | solution.py:21
  97.4 1.3 %collective-permute-done.22 = f32[32,128]{0,1:T(8,128)S(1)} collective-permute-done((f32[32,128]{0,1:T(8,128)S(1)}, f32[32,128]{0,1:T(8,128)S(1)}, u32[]{:S(2)}, u32[]{:S(2)}) %collective-permute-start.22) | collective-permute-done | bytes 16416 | tf_op jit(solution)/shard_map/ppermute | solution.py:21
  98.8 0.7 add_convert_fusion.3
  (100 shorter events, 2.5 us)
Async XLA Ops:
  0.6 18.1 %copy-start = (bf16[256,2048]{1,0:T(8,128)(2,1)S(1)}, bf16[256,2048]{1,0:T(8,128)(2,1)}, u32[]{:S(2)}) copy-start(bf16[256,2048]{1,0:T(8,128)(2,1)} %param.31) | copy-start | bytes 3145732
  0.6 11.3 %copy-start.2 = (bf16[32,2048]{1,0:T(8,128)(2,1)S(1)}, bf16[32,2048]{1,0:T(8,128)(2,1)}, u32[]{:S(2)}) copy-start(bf16[32,2048]{1,0:T(8,128)(2,1)} %param.22) | copy-start | bytes 393220
  0.7 10.3 %copy-start.6 = (f32[32,2,128]{2,1,0:T(2,128)S(1)}, f32[32,2,128]{2,1,0:T(2,128)}, u32[]{:S(2)}) copy-start(f32[32,2,128]{2,1,0:T(2,128)} %param.33) | copy-start | bytes 98308
  0.7 11.2 %copy-start.3 = (bf16[2048,256]{1,0:T(8,128)(2,1)S(1)}, bf16[2048,256]{1,0:T(8,128)(2,1)}, u32[]{:S(2)}) copy-start(bf16[2048,256]{1,0:T(8,128)(2,1)} %param.27) | copy-start | bytes 3145732
  9.1 6.8 %copy-start.8 = (f32[32,2]{0,1:T(2,128)}, f32[32,2]{0,1:T(2,128)S(1)}, u32[]{:S(2)}) copy-start(f32[32,2]{0,1:T(2,128)S(1)} %get-tuple-element.19) | copy-start | bytes 772
  16.0 2.0 %copy-start.1 = (f32[32,2,128,128]{3,2,1,0:T(8,128)}, f32[32,2,128,128]{3,2,1,0:T(8,128)S(1)}, u32[]{:S(2)}) copy-start(f32[32,2,128,128]{3,2,1,0:T(8,128)S(1)} %multiply_add_fusion) | copy-start | bytes 12582916
  18.0 4.2 %copy-start.12 = (s32[32,2]{0,1:T(2,128)S(1)}, s32[32,2]{0,1:T(2,128)}, u32[]{:S(2)}) copy-start(s32[32,2]{0,1:T(2,128)} %param.35) | copy-start | bytes 772
  18.0 4.8 %copy-start.9 = (f32[32,2]{0,1:T(2,128)S(1)}, f32[32,2]{0,1:T(2,128)}, u32[]{:S(2)}) copy-start(f32[32,2]{0,1:T(2,128)} %param.36) | copy-start | bytes 772
  18.0 10.8 %copy-start.7 = (f32[2048]{0:T(1024)S(1)}, f32[2048]{0:T(1024)}, u32[]{:S(2)}) copy-start(f32[2048]{0:T(1024)} %param.43) | copy-start | bytes 24580
  18.6 29.8 %copy-start.4 = (bf16[512,704]{0,1:T(8,128)(2,1)S(1)}, bf16[512,704]{0,1:T(8,128)(2,1)}, u32[]{:S(2)}) copy-start(bf16[512,704]{0,1:T(8,128)(2,1)} %param.40) | copy-start | bytes 2162692
  19.0 29.8 %copy-start.5 = (bf16[512,704]{0,1:T(8,128)(2,1)S(1)}, bf16[512,704]{0,1:T(8,128)(2,1)}, u32[]{:S(2)}) copy-start(bf16[512,704]{0,1:T(8,128)(2,1)} %param.41) | copy-start | bytes 2162692
  19.0 6.4 %collective-permute-start.2 = (bf16[32,2048]{1,0:T(8,128)(2,1)S(1)}, bf16[32,2048]{1,0:T(8,128)(2,1)S(1)}, u32[]{:S(2)}, u32[]{:S(2)}) collective-permute-start(bf16[32,2048]{1,0:T(8,128)(2,1)S(1)} %convolution_convert_fusion), channel_id=1, source_target_pairs={{0,3},{1,2},{2,1},{3,0},{4,7},{5,6},{6,5},{7,4},{8,11},{9,10},{10,... | collective-permute-start | bytes 393224 | tf_op jit(solution)/shard_map/ppermute | solution.py:21
  21.5 6.9 %collective-permute-start.1 = (bf16[32,2048]{1,0:T(8,128)(2,1)S(1)}, bf16[32,2048]{1,0:T(8,128)(2,1)S(1)}, u32[]{:S(2)}, u32[]{:S(2)}) collective-permute-start(bf16[32,2048]{1,0:T(8,128)(2,1)S(1)} %convolution_convert_fusion), channel_id=1, source_target_pairs={{0,2},{1,3},{2,0},{3,1},{4,6},{5,7},{6,4},{7,5},{8,10},{9,11},{10,... | collective-permute-start | bytes 393224 | tf_op jit(solution)/shard_map/ppermute | solution.py:21
  22.1 6.2 %collective-permute-start = (bf16[32,2048]{1,0:T(8,128)(2,1)S(1)}, bf16[32,2048]{1,0:T(8,128)(2,1)S(1)}, u32[]{:S(2)}, u32[]{:S(2)}) collective-permute-start(bf16[32,2048]{1,0:T(8,128)(2,1)S(1)} %convolution_convert_fusion), channel_id=1, source_target_pairs={{0,1},{1,0},{2,3},{3,2},{4,5},{5,4},{6,7},{7,6},{8,9},{9,8},{10,11... | collective-permute-start | bytes 393224 | tf_op jit(solution)/shard_map/ppermute | solution.py:21
  29.3 5.4 %collective-permute-start.3 = (bf16[1,32,640]{2,1,0:T(8,128)(2,1)S(1)}, bf16[1,32,640]{2,1,0:T(8,128)(2,1)S(1)}, u32[]{:S(2)}, u32[]{:S(2)}) collective-permute-start(bf16[1,32,640]{2,1,0:T(8,128)(2,1)S(1)} %fusion.63), channel_id=1, source_target_pairs={{0,16},{4,20},{8,24},{12,28},{16,0},{20,4},{24,8},{28,12},{1,17},{... | collective-permute-start | bytes 122888 | tf_op jit(solution)/shard_map/ppermute | solution.py:21
  34.7 4.5 %collective-permute-start.4 = (bf16[2,32,640]{2,1,0:T(8,128)(2,1)S(1)}, bf16[2,32,640]{2,1,0:T(8,128)(2,1)S(1)}, u32[]{:S(2)}, u32[]{:S(2)}) collective-permute-start(bf16[2,32,640]{2,1,0:T(8,128)(2,1)S(1)} %pad_maximum_fusion.10), channel_id=1, source_target_pairs={{0,8},{4,12},{8,0},{12,4},{16,24},{20,28},{24,16},{28,20},{1,9},{5... | collective-permute-start | bytes 245768 | tf_op jit(solution)/shard_map/ppermute | solution.py:21
  39.3 5.7 %collective-permute-start.5 = (bf16[4,32,640]{2,1,0:T(8,128)(2,1)S(1)}, bf16[4,32,640]{2,1,0:T(8,128)(2,1)S(1)}, u32[]{:S(2)}, u32[]{:S(2)}) collective-permute-start(bf16[4,32,640]{2,1,0:T(8,128)(2,1)S(1)} %pad_maximum_fusion.6), channel_id=1, source_target_pairs={{0,4},{4,0},{8,12},{12,8},{16,20},{20,16},{24,28},{28,24},{1,5},{5... | collective-permute-start | bytes 491528 | tf_op jit(solution)/shard_map/ppermute | solution.py:21
  41.6 6.8 %copy-start.10 = (f32[128]{0:T(128)}, f32[128]{0:T(128)S(1)}, u32[]{:S(2)}) copy-start(f32[128]{0:T(128)S(1)} %iota_convert_fusion) | copy-start | bytes 1540
  46.3 6.2 %collective-permute-start.8 = (bf16[128,512]{1,0:T(8,128)(2,1)}, bf16[128,512]{1,0:T(8,128)(2,1)}, u32[]{:S(2)}, u32[]{:S(2)}) collective-permute-start(bf16[128,512]{1,0:T(8,128)(2,1)} %convolution_convert_fusion.3), channel_id=1, source_target_pairs={{0,3},{1,2},{2,1},{3,0},{4,7},{5,6},{6,5},{7,4},{8,11},{9,10},{10,... | collective-permute-start | bytes 393224 | tf_op jit(solution)/shard_map/ppermute | solution.py:21
  46.3 9.5 %collective-permute-start.7 = (bf16[128,512]{1,0:T(8,128)(2,1)}, bf16[128,512]{1,0:T(8,128)(2,1)}, u32[]{:S(2)}, u32[]{:S(2)}) collective-permute-start(bf16[128,512]{1,0:T(8,128)(2,1)} %convolution_convert_fusion.3), channel_id=1, source_target_pairs={{0,2},{1,3},{2,0},{3,1},{4,6},{5,7},{6,4},{7,5},{8,10},{9,11},{10,... | collective-permute-start | bytes 393224 | tf_op jit(solution)/shard_map/ppermute | solution.py:21
  48.3 7.5 %collective-permute-start.6 = (bf16[128,512]{1,0:T(8,128)(2,1)}, bf16[128,512]{1,0:T(8,128)(2,1)}, u32[]{:S(2)}, u32[]{:S(2)}) collective-permute-start(bf16[128,512]{1,0:T(8,128)(2,1)} %convolution_convert_fusion.3), channel_id=1, source_target_pairs={{0,1},{1,0},{2,3},{3,2},{4,5},{5,4},{6,7},{7,6},{8,9},{9,8},{10,11... | collective-permute-start | bytes 393224 | tf_op jit(solution)/shard_map/ppermute | solution.py:21
  50.2 15.8 %collective-permute-start.14 = (bf16[64,1408]{1,0:T(8,128)(2,1)}, bf16[64,1408]{1,0:T(8,128)(2,1)}, u32[]{:S(2)}, u32[]{:S(2)}) collective-permute-start(bf16[64,1408]{1,0:T(8,128)(2,1)} %get-tuple-element.22), channel_id=1, source_target_pairs={{0,3},{1,2},{2,1},{3,0},{4,7},{5,6},{6,5},{7,4},{8,11},{9,10},{10,... | collective-permute-start | bytes 540680 | tf_op jit(solution)/shard_map/ppermute | solution.py:21
  51.6 14.4 %collective-permute-start.13 = (bf16[64,1408]{1,0:T(8,128)(2,1)}, bf16[64,1408]{1,0:T(8,128)(2,1)}, u32[]{:S(2)}, u32[]{:S(2)}) collective-permute-start(bf16[64,1408]{1,0:T(8,128)(2,1)} %get-tuple-element.21), channel_id=1, source_target_pairs={{0,2},{1,3},{2,0},{3,1},{4,6},{5,7},{6,4},{7,5},{8,10},{9,11},{10,... | collective-permute-start | bytes 540680 | tf_op jit(solution)/shard_map/ppermute | solution.py:21
  52.5 13.5 %collective-permute-start.12 = (bf16[64,1408]{1,0:T(8,128)(2,1)}, bf16[64,1408]{1,0:T(8,128)(2,1)S(1)}, u32[]{:S(2)}, u32[]{:S(2)}) collective-permute-start(bf16[64,1408]{1,0:T(8,128)(2,1)} %get-tuple-element.20), channel_id=1, source_target_pairs={{0,1},{1,0},{2,3},{3,2},{4,5},{5,4},{6,7},{7,6},{8,9},{9,8},{10,11... | collective-permute-start | bytes 540680 | tf_op jit(solution)/shard_map/ppermute | solution.py:21
  65.2 11.5 %copy-start.13 = (bf16[704,512]{1,0:T(8,128)(2,1)S(1)}, bf16[704,512]{1,0:T(8,128)(2,1)}, u32[]{:S(2)}) copy-start(bf16[704,512]{1,0:T(8,128)(2,1)} %param.42) | copy-start | bytes 2162692
  65.2 12.2 %copy-start.11 = (f32[128]{0:T(128)S(1)}, f32[128]{0:T(128)}, u32[]{:S(2)}) copy-start(f32[128]{0:T(128)} %copy-done.10) | copy-start | bytes 1540
  65.3 11.8 %collective-permute-start.11 = (bf16[128,512]{1,0:T(8,128)(2,1)S(1)}, bf16[128,512]{1,0:T(8,128)(2,1)S(1)}, u32[]{:S(2)}, u32[]{:S(2)}) collective-permute-start(bf16[128,512]{1,0:T(8,128)(2,1)S(1)} %get-tuple-element.24), channel_id=1, source_target_pairs={{0,3},{1,2},{2,1},{3,0},{4,7},{5,6},{6,5},{7,4},{8,11},{9,10},{10,... | collective-permute-start | bytes 393224 | tf_op jit(solution)/shard_map/ppermute | solution.py:21
  65.3 11.7 %collective-permute-start.10 = (bf16[128,512]{1,0:T(8,128)(2,1)S(1)}, bf16[128,512]{1,0:T(8,128)(2,1)S(1)}, u32[]{:S(2)}, u32[]{:S(2)}) collective-permute-start(bf16[128,512]{1,0:T(8,128)(2,1)S(1)} %get-tuple-element.25), channel_id=1, source_target_pairs={{0,2},{1,3},{2,0},{3,1},{4,6},{5,7},{6,4},{7,5},{8,10},{9,11},{10,... | collective-permute-start | bytes 393224 | tf_op jit(solution)/shard_map/ppermute | solution.py:21
  67.3 8.8 %collective-permute-start.17 = (bf16[64,704]{1,0:T(8,128)(2,1)S(1)}, bf16[64,704]{1,0:T(8,128)(2,1)S(1)}, u32[]{:S(2)}, u32[]{:S(2)}) collective-permute-start(bf16[64,704]{1,0:T(8,128)(2,1)S(1)} %fusion.41), channel_id=1, source_target_pairs={{0,3},{1,2},{2,1},{3,0},{4,7},{5,6},{6,5},{7,4},{8,11},{9,10},{10,... | collective-permute-start | bytes 270344 | tf_op jit(solution)/shard_map/ppermute | solution.py:21
  68.4 8.1 %collective-permute-start.16 = (bf16[64,704]{1,0:T(8,128)(2,1)S(1)}, bf16[64,704]{1,0:T(8,128)(2,1)S(1)}, u32[]{:S(2)}, u32[]{:S(2)}) collective-permute-start(bf16[64,704]{1,0:T(8,128)(2,1)S(1)} %fusion.41), channel_id=1, source_target_pairs={{0,2},{1,3},{2,0},{3,1},{4,6},{5,7},{6,4},{7,5},{8,10},{9,11},{10,... | collective-permute-start | bytes 270344 | tf_op jit(solution)/shard_map/ppermute | solution.py:21
  70.2 6.4 %collective-permute-start.15 = (bf16[64,704]{1,0:T(8,128)(2,1)S(1)}, bf16[64,704]{1,0:T(8,128)(2,1)S(1)}, u32[]{:S(2)}, u32[]{:S(2)}) collective-permute-start(bf16[64,704]{1,0:T(8,128)(2,1)S(1)} %fusion.41), channel_id=1, source_target_pairs={{0,1},{1,0},{2,3},{3,2},{4,5},{5,4},{6,7},{7,6},{8,9},{9,8},{10,11... | collective-permute-start | bytes 270344 | tf_op jit(solution)/shard_map/ppermute | solution.py:21
  76.0 1.3 %collective-permute-start.9 = (bf16[128,512]{1,0:T(8,128)(2,1)S(1)}, bf16[128,512]{1,0:T(8,128)(2,1)S(1)}, u32[]{:S(2)}, u32[]{:S(2)}) collective-permute-start(bf16[128,512]{1,0:T(8,128)(2,1)S(1)} %get-tuple-element.23), channel_id=1, source_target_pairs={{0,1},{1,0},{2,3},{3,2},{4,5},{5,4},{6,7},{7,6},{8,9},{9,8},{10,11... | collective-permute-start | bytes 393224 | tf_op jit(solution)/shard_map/ppermute | solution.py:21
  77.8 6.4 %collective-permute-start.18 = (bf16[4,32,512]{2,1,0:T(8,128)(2,1)S(1)}, bf16[4,32,512]{2,1,0:T(8,128)(2,1)S(1)}, u32[]{:S(2)}, u32[]{:S(2)}) collective-permute-start(bf16[4,32,512]{2,1,0:T(8,128)(2,1)S(1)} %bitcast.120), channel_id=1, source_target_pairs={{0,4},{4,0},{8,12},{12,8},{16,20},{20,16},{24,28},{28,24},{1,5},{5... | collective-permute-start | bytes 393224 | tf_op jit(solution)/shard_map/ppermute | solution.py:21
  84.3 4.3 %collective-permute-start.19 = (bf16[2,32,512]{2,1,0:T(8,128)(2,1)S(1)}, bf16[2,32,512]{2,1,0:T(8,128)(2,1)S(1)}, u32[]{:S(2)}, u32[]{:S(2)}) collective-permute-start(bf16[2,32,512]{2,1,0:T(8,128)(2,1)S(1)} %slice.149), channel_id=1, source_target_pairs={{0,8},{4,12},{8,0},{12,4},{16,24},{20,28},{24,16},{28,20},{1,9},{5... | collective-permute-start | bytes 196616 | tf_op jit(solution)/shard_map/ppermute | solution.py:21
  88.6 4.9 %collective-permute-start.20 = (bf16[1,32,512]{2,1,0:T(8,128)(2,1)S(1)}, bf16[1,32,512]{2,1,0:T(8,128)(2,1)S(1)}, u32[]{:S(2)}, u32[]{:S(2)}) collective-permute-start(bf16[1,32,512]{2,1,0:T(8,128)(2,1)S(1)} %slice.150), channel_id=1, source_target_pairs={{0,16},{4,20},{8,24},{12,28},{16,0},{20,4},{24,8},{28,12},{1,17},{... | collective-permute-start | bytes 98312 | tf_op jit(solution)/shard_map/ppermute | solution.py:21
  93.6 3.8 %collective-permute-start.23 = (f32[32,128]{0,1:T(8,128)S(1)}, f32[32,128]{0,1:T(8,128)S(1)}, u32[]{:S(2)}, u32[]{:S(2)}) collective-permute-start(f32[32,128]{0,1:T(8,128)S(1)} %broadcast_in_dim.9), channel_id=1, source_target_pairs={{0,3},{1,2},{2,1},{3,0},{4,7},{5,6},{6,5},{7,4},{8,11},{9,10},{10,... | collective-permute-start | bytes 49160 | tf_op jit(solution)/shard_map/ppermute | solution.py:21
  93.7 5.0 %collective-permute-start.22 = (f32[32,128]{0,1:T(8,128)S(1)}, f32[32,128]{0,1:T(8,128)S(1)}, u32[]{:S(2)}, u32[]{:S(2)}) collective-permute-start(f32[32,128]{0,1:T(8,128)S(1)} %broadcast_in_dim.9), channel_id=1, source_target_pairs={{0,2},{1,3},{2,0},{3,1},{4,6},{5,7},{6,4},{7,5},{8,10},{9,11},{10,... | collective-permute-start | bytes 49160 | tf_op jit(solution)/shard_map/ppermute | solution.py:21
  93.8 5.0 %collective-permute-start.21 = (f32[32,128]{0,1:T(8,128)S(1)}, f32[32,128]{0,1:T(8,128)S(1)}, u32[]{:S(2)}, u32[]{:S(2)}) collective-permute-start(f32[32,128]{0,1:T(8,128)S(1)} %broadcast_in_dim.9), channel_id=1, source_target_pairs={{0,1},{1,0},{2,3},{3,2},{4,5},{5,4},{6,7},{7,6},{8,9},{9,8},{10,11... | collective-permute-start | bytes 49160 | tf_op jit(solution)/shard_map/ppermute | solution.py:21
